TPU v7x, 32 devices: a whole 2x2x4 slice. The times are simulated.
32 devices in a mesh: fs: 8 (over z, y), tp: 4 (over x, core).
Axes of the slice: x: 2, y: 2, z: 4, core: 2. Of those that a mesh axis runs over, the one named last changes fastest.
Arguments:
- normed_input: bfloat16 [36864, 2048], P('fs'), may hold values from -8 to 8
- query_latent_cotangent: bfloat16 [36864, 768], P('fs', 'tp'), may hold values from -0.03125 to 0.03125
- key_value_latent_cotangent: bfloat16 [36864, 512], P('fs', 'tp'), may hold values from -0.03125 to 0.03125
- row_factor: bfloat16 [2048, 256], P('fs'), may hold values from -0.1875 to 0.1875
- query_down_weight: float32 [2048, 768], P('fs', 'tp'), may hold values from -6 to 6
- key_value_down_weight: float32 [2048, 512], P('fs', 'tp'), may hold values from -6 to 6
- query_first_moment: float32 [256, 768], P('fs', 'tp'), may hold values from -6 to 6
- key_value_first_moment: float32 [256, 512], P('fs', 'tp'), may hold values from -6 to 6
- query_second: float32 [256, 768], P('fs', 'tp'), may hold values from 0.5 to 2000
- latent_second: float32 [256, 512], P('fs', 'tp'), may hold values from 0.5 to 2000
Outputs:
- query_new: float32 [2048, 768], P('fs', 'tp')
- latent_new: float32 [2048, 512], P('fs', 'tp')
- query_step: float32 [2048, 768], P('fs', 'tp')
- latent_step: float32 [2048, 512], P('fs', 'tp')
- query_copy: bfloat16 [2048, 768], P(None, 'tp')
- latent_copy: bfloat16 [2048, 512], P(None, 'tp')
- query_first_new: float32 [256, 768], P('fs', 'tp')
- latent_first_new: float32 [256, 512], P('fs', 'tp')
- query_second_new: float32 [256, 768], P('fs', 'tp')
- latent_second_new: float32 [256, 512], P('fs', 'tp')
All inputs are finite; a program needn't handle non-finite values.
Results may differ from a plain program's by a relative error of at most 0.006.
Values may be sent and summed in bfloat16 or wider, within the bound.
A program may use at most 64 MiB of HBM per device.

v0:
```python
import jax
import jax.numpy as jnp
from jax import lax
from jax.sharding import PartitionSpec as P


def token_sum(left, right):
    return lax.dot_general(
        left, right, (((0,), (0,)), ((), ())), preferred_element_type=jnp.float32
    )


def moment_update(projected, first, second):
    first_new = 0.8 * first + 0.2 * projected
    second_new = 0.9 * second + 0.1 * projected * projected
    direction = first_new / (jnp.sqrt(second_new) + 1e-08)
    return (first_new, second_new, direction)


def body(
    normed_input,
    query_latent_cotangent,
    key_value_latent_cotangent,
    row_factor,
    query_down_weight,
    key_value_down_weight,
    query_first_moment,
    key_value_first_moment,
    query_second,
    latent_second,
):
    fs_count = lax.axis_size("fs")
    tp_count = lax.axis_size("tp")
    query_width = query_latent_cotangent.shape[1]
    rank_rows = query_first_moment.shape[0]
    factor_whole = lax.all_gather(row_factor, "fs", axis=0, tiled=True)
    latent_tokens = jnp.dot(normed_input, factor_whole, preferred_element_type=jnp.float32)
    upper_part = latent_tokens.astype(jnp.bfloat16)
    lower_part = (latent_tokens - upper_part.astype(jnp.float32)).astype(jnp.bfloat16)
    both_cotangents = jnp.concatenate([query_latent_cotangent, key_value_latent_cotangent], axis=1)
    projected = lax.psum_scatter(
        (token_sum(upper_part, both_cotangents) + token_sum(lower_part, both_cotangents)).astype(
            jnp.bfloat16
        ),
        "fs",
        scatter_dimension=0,
        tiled=True,
    ).astype(jnp.float32)
    query_first_new, query_second_new, query_dir = moment_update(
        projected[:, :query_width], query_first_moment, query_second
    )
    latent_first_new, latent_second_new, latent_dir = moment_update(
        projected[:, query_width:], key_value_first_moment, latent_second
    )
    query_sq, latent_sq = lax.psum(
        (jnp.sum(query_dir * query_dir), jnp.sum(latent_dir * latent_dir)), ("fs", "tp")
    )
    query_count = rank_rows * fs_count * query_width * tp_count
    latent_count = rank_rows * fs_count * key_value_latent_cotangent.shape[1] * tp_count
    query_scale = 0.5 * jnp.sqrt(jnp.float32(query_count)) / jnp.sqrt(query_sq + 1e-06)
    latent_scale = 0.5 * jnp.sqrt(jnp.float32(latent_count)) / jnp.sqrt(latent_sq + 1e-06)
    scaled = jnp.concatenate([query_scale * query_dir, latent_scale * latent_dir], axis=1)
    factor_rows = row_factor.astype(jnp.float32)
    steps = jnp.dot(
        factor_rows,
        lax.all_gather(scaled, "fs", axis=0, tiled=True),
        precision=lax.Precision.HIGHEST,
        preferred_element_type=jnp.float32,
    )
    query_step = steps[:, :query_width]
    latent_step = steps[:, query_width:]
    query_new = query_down_weight - query_step
    latent_new = key_value_down_weight - latent_step
    query_copy, latent_copy = (
        lax.all_gather(query_new.astype(jnp.bfloat16), "fs", axis=0, tiled=True),
        lax.all_gather(latent_new.astype(jnp.bfloat16), "fs", axis=0, tiled=True),
    )
    return (
        query_new,
        latent_new,
        query_step,
        latent_step,
        query_copy,
        latent_copy,
        query_first_new,
        latent_first_new,
        query_second_new,
        latent_second_new,
    )


def solution(mesh):
    in_specs = (
        P("fs", None),
        P("fs", "tp"),
        P("fs", "tp"),
        P("fs", None),
        P("fs", "tp"),
        P("fs", "tp"),
        P("fs", "tp"),
        P("fs", "tp"),
        P("fs", "tp"),
        P("fs", "tp"),
    )
    out_specs = (
        P("fs", "tp"),
        P("fs", "tp"),
        P("fs", "tp"),
        P("fs", "tp"),
        P(None, "tp"),
        P(None, "tp"),
        P("fs", "tp"),
        P("fs", "tp"),
        P("fs", "tp"),
        P("fs", "tp"),
    )
    return jax.shard_map(body, mesh=mesh, in_specs=in_specs, out_specs=out_specs, check_vma=False)
```

profile of v0, /device:TPU:0, one launch (start us, length us, event | category | flops | bytes accessed | tf_op | source)
XLA Modules:
  0.0 277.1 jit_solution(13795625494612801847)
XLA Ops:
  7.2 0.0 all-gather.2.cloned.1.call-start
  7.2 0.7 all-gather.2.cloned.1.call-update
  7.9 0.0 reduce-scatter.2.cloned.1.call-start
  8.0 1.6 copy.20
  9.5 0.0 copy-start
  9.5 43.6 %all-gather.2.cloned.1.call-done = bf16[2048,256]{1,0:T(8,128)(2,1)} async-done(((bf16[256,256]{1,0:T(8,128)(2,1)}), bf16[2048,256]{1,0:T(8,128)(2,1)}) %all-gather.2.cloned.1.call-update) | async-done | bytes 1048592 | tf_op jit(solution)/shard_map/all_gather | solution.py:36
  53.1 9.5 %fusion.16 = f32[4608,256]{1,0:T(8,128)S(1)} fusion(bf16[4608,2048]{1,0:T(8,128)(2,1)} %param.10, bf16[2048,256]{1,0:T(8,128)(2,1)} %all-gather.2.cloned.1.call-done), kind=kOutput, calls=%fused_computation.27 | convolution fusion | flops 4831838208 | bytes 24641536 | tf_op jit(solution)/shard_map/dot_general | solution.py:37
  62.7 0.0 copy-done
  62.7 1.5 fusion
  64.2 0.0 copy-start.5
  64.2 0.0 copy-start.8
  64.2 0.0 copy-start.9
  64.2 0.0 copy-start.10
  64.2 0.0 copy-start.11
  64.3 0.0 copy-start.1
  64.3 0.0 copy-start.2
  64.3 2.2 fusion.5
  66.5 0.0 reduce-scatter.2.cloned.1.call-update
  66.5 0.0 copy-done.5
  66.5 0.1 copy.21
  66.6 60.7 %reduce-scatter.2.cloned.1.call-done = bf16[32,320]{1,0:T(8,128)(2,1)} async-done(((bf16[256,320]{1,0:T(8,128)(2,1)}), bf16[32,320]{1,0:T(8,128)(2,1)}) %reduce-scatter.2.cloned.1.call-update) | async-done | bytes 20496 | tf_op jit(solution)/shard_map/reduce_scatter | solution.py:41
  127.3 0.7 convert_element_type.26
  128.0 0.0 copy-done.8
  128.0 0.0 copy-done.9
  128.1 0.6 multiply_reduce_fusion
  128.7 0.0 copy-done.10
  128.7 0.0 copy-done.11
  128.7 0.0 copy-start.3
  128.7 0.0 copy-start.4
  128.7 0.7 multiply_reduce_fusion.1
  129.4 0.0 copy-start.6
  129.4 0.0 copy-start.7
  129.4 40.3 %all-reduce = (f32[]{:T(128)}, f32[]{:T(128)}) all-reduce(f32[]{:T(128)} %get-tuple-element.30, f32[]{:T(128)} %get-tuple-element.27), channel_id=1, replica_groups=mesh['fs'=8,'tp'=4] {'fs','tp'}, use_global_device_ids=true, to_apply=%region_4.0 | all-reduce | flops 2 | bytes 16 | tf_op jit(solution)/shard_map/psum | solution.py:55
  171.2 0.1 pad_maximum_fusion.7
  171.2 31.0 %all_gather.13 = f32[256,320]{1,0:T(8,128)S(1)} all-gather(f32[32,320]{1,0:T(8,128)S(1)} %pad_maximum_fusion.7), channel_id=1, replica_groups=mesh['fs'=8,'tp'=4] {'fs'}, dimensions={0}, use_global_device_ids=true | all-gather | bytes 368640 | tf_op jit(solution)/shard_map/all_gather | solution.py:66
  202.2 0.0 copy-done.1
  202.2 0.5 convolution_bitcast_fusion
  202.7 0.0 copy-done.2
  202.7 0.8 fusion.13
  203.5 32.2 %all_gather.14 = bf16[2048,192]{0,1:T(8,128)(2,1)S(1)} all-gather(bf16[256,192]{0,1:T(8,128)(2,1)S(1)} %get-tuple-element.24), channel_id=1, replica_groups=mesh['fs'=8,'tp'=4] {'fs'}, dimensions={0}, use_global_device_ids=true | all-gather | bytes 884736 | tf_op jit(solution)/shard_map/all_gather | solution.py:75
  235.7 31.2 %all_gather.15 = bf16[2048,128]{0,1:T(8,128)(2,1)S(1)} all-gather(bf16[256,128]{0,1:T(8,128)(2,1)S(1)} %get-tuple-element.22), channel_id=1, replica_groups=mesh['fs'=8,'tp'=4] {'fs'}, dimensions={0}, use_global_device_ids=true | all-gather | bytes 589824 | tf_op jit(solution)/shard_map/all_gather | solution.py:76
  266.9 1.0 copy.24
  267.9 0.8 copy.22
  268.7 0.0 copy-done.3
  268.7 0.0 copy-done.4
  268.7 0.8 copy.23
  269.4 0.0 copy-done.6
  269.4 0.0 copy-done.7
  269.4 0.9 copy.26
  (3 shorter events, 0.1 us)
Async XLA Ops:
  7.2 46.0 %all-gather.2.cloned.1.call-start = ((), (), s32[]{:S(2)}) async-start(), calls=%async_computation.1 | async-start | bytes 1179648 | tf_op jit(solution)/shard_map/all_gather | solution.py:36
  7.9 119.4 %reduce-scatter.2.cloned.1.call-start = ((), (), s32[]{:S(2)}) async-start(), calls=%async_computation.2 | async-start | bytes 221184 | tf_op jit(solution)/shard_map/reduce_scatter | solution.py:41
  9.5 53.1 %copy-start = (bf16[4608,192]{0,1:T(8,128)(2,1)S(1)}, bf16[4608,192]{0,1:T(8,128)(2,1)}, u32[]{:S(2)}) copy-start(bf16[4608,192]{0,1:T(8,128)(2,1)} %param.11) | copy-start | bytes 5308420
  64.2 2.3 copy-start.5
  64.2 63.8 %copy-start.8 = (f32[32,192]{1,0:T(8,128)S(1)}, f32[32,192]{1,0:T(8,128)}, u32[]{:S(2)}) copy-start(f32[32,192]{1,0:T(8,128)} %param.18) | copy-start | bytes 73732
  64.2 63.8 %copy-start.9 = (f32[32,192]{1,0:T(8,128)S(1)}, f32[32,192]{1,0:T(8,128)}, u32[]{:S(2)}) copy-start(f32[32,192]{1,0:T(8,128)} %param.16) | copy-start | bytes 73732
  64.2 64.5 %copy-start.10 = (f32[32,128]{1,0:T(8,128)S(1)}, f32[32,128]{1,0:T(8,128)}, u32[]{:S(2)}) copy-start(f32[32,128]{1,0:T(8,128)} %param.19) | copy-start | bytes 49156
  64.2 64.4 %copy-start.11 = (f32[32,128]{1,0:T(8,128)S(1)}, f32[32,128]{1,0:T(8,128)}, u32[]{:S(2)}) copy-start(f32[32,128]{1,0:T(8,128)} %param.17) | copy-start | bytes 49156
  64.3 138.0 %copy-start.1 = (bf16[256,256]{1,0:T(8,128)(2,1)S(1)}, bf16[256,256]{1,0:T(8,128)(2,1)}, u32[]{:S(2)}) copy-start(bf16[256,256]{1,0:T(8,128)(2,1)} %param.13) | copy-start | bytes 393220
  64.3 138.4 %copy-start.2 = (f32[256,192]{0,1:T(8,128)S(1)}, f32[256,192]{0,1:T(8,128)}, u32[]{:S(2)}) copy-start(f32[256,192]{0,1:T(8,128)} %param.14) | copy-start | bytes 589828
  128.7 140.0 %copy-start.3 = (f32[32,192]{1,0:T(8,128)}, f32[32,192]{1,0:T(8,128)S(1)}, u32[]{:S(2)}) copy-start(f32[32,192]{1,0:T(8,128)S(1)} %get-tuple-element.52) | copy-start | bytes 73732
  128.7 140.0 %copy-start.4 = (f32[32,192]{1,0:T(8,128)}, f32[32,192]{1,0:T(8,128)S(1)}, u32[]{:S(2)}) copy-start(f32[32,192]{1,0:T(8,128)S(1)} %get-tuple-element.50) | copy-start | bytes 73732
  129.4 140.0 %copy-start.6 = (f32[32,128]{1,0:T(8,128)}, f32[32,128]{1,0:T(8,128)S(1)}, u32[]{:S(2)}) copy-start(f32[32,128]{1,0:T(8,128)S(1)} %get-tuple-element.53) | copy-start | bytes 49156
  129.4 140.0 %copy-start.7 = (f32[32,128]{1,0:T(8,128)}, f32[32,128]{1,0:T(8,128)S(1)}, u32[]{:S(2)}) copy-start(f32[32,128]{1,0:T(8,128)S(1)} %get-tuple-element.51) | copy-start | bytes 49156
Sparse Core Ops, SparseCore 0:
  10.1 42.9 all-gather.1
  66.6 60.6 reduce-scatter.1
where the time goes:
time: 278 us; the launch traced here: 277 us
  blocking collectives  135 us (49%)
  waiting for transfers between devices  105 us (38%)
  between operations  15.6 us (6%)
  matrix products  13.7 us (5%)
  local copies, waits for them, and re-layouts  5.12 us (2%)
  other arithmetic  2.98 us (1%)
    reduce_scatter x1, waiting for transfers between devices, body(): lax.psum_scatter((token_sum(upper_part, both_cotangents) + token_sum(lowe...  60.7 us
    all_gather x1, waiting for transfers between devices, body(): factor_whole = lax.all_gather(row_factor, 'fs', axis=0, tiled=True)  43.6 us
    psum x1, blocking collectives, body(): lax.psum((jnp.sum(query_dir * query_dir), jnp.sum(latent_dir * latent_dir...  40.3 us
    all_gather x1, blocking collectives, body(): lax.all_gather(query_new.astype(jnp.bfloat16), 'fs', axis=0, tiled=True)  32.2 us
    all_gather x1, blocking collectives, body(): lax.all_gather(latent_new.astype(jnp.bfloat16), 'fs', axis=0, tiled=True)  31.2 us
    all_gather x1, blocking collectives, body(): lax.all_gather(scaled, 'fs', axis=0, tiled=True)  31 us
    dot_general x1, matrix products, body(): jnp.dot(normed_input, factor_whole, preferred_element_type=jnp.float32)  9.51 us
  transfers between devices with their start and end apart: 2, of which 2 were waited for; matrix products, arithmetic and copies ran while one was open for 1% of the time, Pallas kernels for 0%

commit v1 on v0

v1 whole, which is shorter than its diff:
```python
import functools

import jax
import jax.numpy as jnp
from jax import lax
from jax.experimental import pallas as pl
from jax.experimental.pallas import tpu as pltpu
from jax.sharding import PartitionSpec as P

MESH = pl.DeviceIdType.MESH
F32 = jnp.float32
BF16 = jnp.bfloat16


def kernel(
    n,
    tp,
    chunks,
    x_hbm,
    cq_hbm,
    ck_hbm,
    p_hbm,
    wq_ref,
    wk_ref,
    mq_ref,
    mk_ref,
    vq_ref,
    vk_ref,
    qnew_ref,
    knew_ref,
    qstep_ref,
    kstep_ref,
    qcopy_ref,
    kcopy_ref,
    qfirst_ref,
    kfirst_ref,
    qsecond_ref,
    ksecond_ref,
    xs,
    cqs,
    cks,
    acc,
    pall,
    wall,
    rs_mine,
    rs_send,
    rs_recv,
    dall,
    sums,
    x_sem,
    c_sem,
    p_local,
    p_send,
    p_recv,
    s_send,
    s_recv,
    w_send,
    w_recv,
    rs_ssem,
    rs_rsem,
    d_send,
    d_recv,
    q_send,
    q_recv,
):
    f = lax.axis_index("fs")
    t = lax.axis_index("tp")
    depth = n // 2
    col, side = f // 2, f % 2
    half = t % 2
    sibling = t + 1 - 2 * half
    across = f + 1 - 2 * side
    me = f * tp + t
    qw = wq_ref.shape[1]
    kw = wk_ref.shape[1]
    rr = mq_ref.shape[0]
    rows = wq_ref.shape[0]

    barrier = pltpu.get_barrier_semaphore()
    for i in range(n):
        for j in range(tp):
            if i or j:
                pl.semaphore_signal(
                    barrier,
                    inc=1,
                    device_id=(lax.rem(f + i, n), lax.rem(t + j, tp)),
                    device_id_type=MESH,
                )

    p_copy = pltpu.make_async_copy(p_hbm, pall.at[f], p_local)
    p_copy.start()
    cq_copy = pltpu.make_async_copy(cq_hbm, cqs, c_sem.at[0])
    ck_copy = pltpu.make_async_copy(ck_hbm, cks, c_sem.at[1])
    cq_copy.start()
    ck_copy.start()

    def x_copy(i):
        return pltpu.make_async_copy(x_hbm.at[i], xs.at[i], x_sem.at[i])

    for i in range(chunks):
        x_copy(i).start()

    wall[f] = jnp.concatenate([wq_ref[...], wk_ref[...]], axis=1).astype(BF16)
    acc[...] = jnp.zeros_like(acc)

    def remote(src, dst, ssem, rsem, to):
        return pltpu.make_async_remote_copy(
            src_ref=src, dst_ref=dst, send_sem=ssem, recv_sem=rsem, device_id=to, device_id_type=MESH
        )

    def p_fs(block, slot, to):
        ref = pall.at[block, half]
        return remote(ref, ref, p_send.at[slot], p_recv.at[block], (to, t))

    def p_tp(block, slot):
        ref = pall.at[block, half]
        return remote(ref, ref, s_send.at[slot], s_recv.at[block], (f, sibling))

    def w_fs(block, slot, to):
        ref = wall.at[block]
        return remote(ref, ref, w_send.at[slot], w_recv.at[block], (to, t))

    def column(k):
        return lax.rem(col + k, depth) * 2 + side

    def other(k):
        return lax.rem(col + k, depth) * 2 + 1 - side

    sends = []

    def go(copy):
        copy.start()
        sends.append(copy)

    def multiply(i, carry):
        x_copy(i).wait()
        left = jnp.concatenate([cqs[i].T, cks[i].T], axis=0)
        acc[...] += jnp.dot(left, xs[i], preferred_element_type=F32)
        return carry

    p_copy.wait()
    pl.semaphore_wait(barrier, n * tp - 1)
    for k in range(1, depth):
        go(p_fs(f, k - 1, column(k)))
    go(p_fs(f, depth - 1, across))
    go(w_fs(f, 0, across))
    if depth > 1:
        go(w_fs(f, 1, column(1)))

    cq_copy.wait()
    ck_copy.wait()
    first = (2 * chunks) // 3
    lax.fori_loop(0, first, multiply, 0)
    slot = depth
    for k in range(depth - 1, 0, -1):
        block = column(k)
        p_fs(block, 0, across).wait_recv()
        go(p_fs(block, slot, across))
        slot += 1
        go(p_tp(block, k))
    lax.fori_loop(first, chunks, multiply, 0)
    for k in range(depth):
        block = other(k)
        p_fs(block, 0, across).wait_recv()
        go(p_tp(block, depth + k))
    for k in range(depth):
        if k > 0:
            remote(pall.at[column(k), 1 - half], pall.at[column(k), 1 - half], s_send.at[0], s_recv.at[column(k)], (f, sibling)).wait_recv()
        remote(pall.at[other(k), 1 - half], pall.at[other(k), 1 - half], s_send.at[0], s_recv.at[other(k)], (f, sibling)).wait_recv()

    whole_p = pall[...].reshape(n * rows, pall.shape[-1])
    projected = jnp.dot(acc[...].astype(BF16), whole_p, preferred_element_type=F32).T
    for k in range(n):
        piece = projected[k * rr : (k + 1) * rr]
        rs_mine[k] = piece
        rs_send[k] = piece.astype(BF16)
    for k in range(1, n):
        to = lax.rem(f + k, n)
        go(remote(rs_send.at[to], rs_recv.at[f], rs_ssem.at[k], rs_rsem.at[f], (to, t)))
    total = rs_mine[f]
    for k in range(1, n):
        src = lax.rem(f + n - k, n)
        remote(rs_recv.at[src], rs_recv.at[src], rs_ssem.at[0], rs_rsem.at[src], (f, sibling)).wait_recv()
        total = total + rs_recv[src].astype(F32)

    def moment_update(part, first_ref, second_ref, first_out, second_out):
        first_new = 0.8 * first_ref[...] + 0.2 * part
        second_new = 0.9 * second_ref[...] + 0.1 * part * part
        first_out[...] = first_new
        second_out[...] = second_new
        return first_new / (jnp.sqrt(second_new) + 1e-08)

    dir_q = moment_update(total[:, :qw], mq_ref, vq_ref, qfirst_ref, qsecond_ref)
    dir_k = moment_update(total[:, qw:], mk_ref, vk_ref, kfirst_ref, ksecond_ref)
    dall[f] = jnp.concatenate([dir_q, dir_k], axis=1).astype(BF16)
    lane = lax.broadcasted_iota(jnp.int32, (1, 128), 1)
    sums[me] = jnp.where(lane < 64, jnp.sum(dir_q * dir_q), jnp.sum(dir_k * dir_k))
    for k in range(1, n):
        to = lax.rem(f + k, n)
        go(remote(dall.at[f], dall.at[f], d_send.at[k], d_recv.at[f], (to, t)))
    for i in range(n):
        for j in range(tp):
            if i or j:
                to = (lax.rem(f + i, n), lax.rem(t + j, tp))
                go(remote(sums.at[me], sums.at[me], q_send.at[i * tp + j], q_recv.at[me], to))

    for k in range(2, depth):
        go(w_fs(f, k, column(k)))
    slot = depth
    for k in range(depth - 1, 0, -1):
        block = column(k)
        w_fs(block, 0, across).wait_recv()
        go(w_fs(block, slot, across))
        slot += 1

    for k in range(1, n):
        src = lax.rem(f + n - k, n)
        remote(dall.at[src], dall.at[src], d_send.at[0], d_recv.at[src], (f, sibling)).wait_recv()
    for i in range(n):
        for j in range(tp):
            if i or j:
                src = lax.rem(f + i, n) * tp + lax.rem(t + j, tp)
                remote(sums.at[src], sums.at[src], q_send.at[0], q_recv.at[src], (f, sibling)).wait_recv()
    row = jnp.sum(sums[...], axis=0)
    q_sq = row[:, 0:1]
    k_sq = row[:, 64:65]
    q_count = jnp.float32(n * rr * qw * tp)
    k_count = jnp.float32(n * rr * kw * tp)
    q_scale = 0.5 * jnp.sqrt(q_count) / jnp.sqrt(q_sq + 1e-06)
    k_scale = 0.5 * jnp.sqrt(k_count) / jnp.sqrt(k_sq + 1e-06)
    lanes = lax.broadcasted_iota(jnp.int32, (1, qw + kw), 1)
    scale = jnp.where(lanes < qw, q_scale, k_scale)
    dirs = jnp.concatenate([dall[k].astype(F32) for k in range(n)], axis=0).astype(BF16)
    mine = pall[f].reshape(rows, pall.shape[-1])
    step = jnp.dot(mine, dirs, preferred_element_type=F32) * scale
    qstep_ref[...] = step[:, :qw]
    kstep_ref[...] = step[:, qw:]
    qnew_ref[...] = wq_ref[...] - step[:, :qw]
    knew_ref[...] = wk_ref[...] - step[:, qw:]

    for k in range(depth):
        block = other(k)
        w_fs(block, 0, across).wait_recv()

    def finish(i, carry):
        step = jnp.dot(pall[i].reshape(rows, pall.shape[-1]), dirs, preferred_element_type=F32) * scale
        new = wall[i].astype(F32) - step
        at = pl.ds(pl.multiple_of(i * rows, rows), rows)
        qcopy_ref[at, :] = new[:, :qw].astype(BF16)
        kcopy_ref[at, :] = new[:, qw:].astype(BF16)
        return carry

    lax.fori_loop(0, n, finish, 0)
    for copy in sends:
        copy.wait_send()


def solution(mesh):
    n, tp = mesh.shape["fs"], mesh.shape["tp"]

    def body(x, cq, ck, factor, wq, wk, mq, mk, vq, vk):
        tokens, width = x.shape
        rows, rank = factor.shape
        qw, kw = wq.shape[1], wk.shape[1]
        lat = qw + kw
        rr = mq.shape[0]
        chunk = 512
        while tokens % chunk:
            chunk //= 2
        chunks = tokens // chunk
        vmem = pl.BlockSpec(memory_space=pltpu.VMEM)
        anys = pl.BlockSpec(memory_space=pl.ANY)
        dma = pltpu.SemaphoreType.DMA
        sds = jax.ShapeDtypeStruct
        return pl.pallas_call(
            functools.partial(kernel, n, tp, chunks),
            out_shape=(
                sds((rows, qw), F32),
                sds((rows, kw), F32),
                sds((rows, qw), F32),
                sds((rows, kw), F32),
                sds((n * rows, qw), BF16),
                sds((n * rows, kw), BF16),
                sds((rr, qw), F32),
                sds((rr, kw), F32),
                sds((rr, qw), F32),
                sds((rr, kw), F32),
            ),
            in_specs=[anys] * 4 + [vmem] * 6,
            out_specs=(vmem,) * 10,
            scratch_shapes=[
                pltpu.VMEM((chunks, chunk, width), BF16),
                pltpu.VMEM((chunks, chunk, qw), BF16),
                pltpu.VMEM((chunks, chunk, kw), BF16),
                pltpu.VMEM((lat, width), F32),
                pltpu.VMEM((n, 2, rows // 2, rank), BF16),
                pltpu.VMEM((n, rows, lat), BF16),
                pltpu.VMEM((n, rr, lat), F32),
                pltpu.VMEM((n, rr, lat), BF16),
                pltpu.VMEM((n, rr, lat), BF16),
                pltpu.VMEM((n, rr, lat), BF16),
                pltpu.VMEM((n * tp, 1, 128), F32),
                dma((chunks,)),
                dma((2,)),
                dma(()),
                dma((n,)),
                dma((n,)),
                dma((n,)),
                dma((n,)),
                dma((n,)),
                dma((n,)),
                dma((n,)),
                dma((n,)),
                dma((n,)),
                dma((n,)),
                dma((n * tp,)),
                dma((n * tp,)),
            ],
            compiler_params=pltpu.CompilerParams(
                collective_id=0, has_side_effects=True, vmem_limit_bytes=58 * 1024 * 1024
            ),
        )(
            x.reshape(chunks, chunk, width),
            cq.reshape(chunks, chunk, qw),
            ck.reshape(chunks, chunk, kw),
            factor.reshape(2, rows // 2, rank),
            wq,
            wk,
            mq,
            mk,
            vq,
            vk,
        )

    return jax.shard_map(
        body,
        mesh=mesh,
        in_specs=(P("fs", None), P("fs", "tp"), P("fs", "tp"), P("fs", None)) + (P("fs", "tp"),) * 6,
        out_specs=(P("fs", "tp"),) * 4 + (P(None, "tp"),) * 2 + (P("fs", "tp"),) * 4,
        check_vma=False,
    )
```

time: 278 us -> 79.8 us (0.29)
  blocking collectives: 135 us -> 0 us
  waiting for transfers between devices: 105 us -> 0 us
  Pallas kernels: 0 us -> 62 us
  between operations: 15.6 us -> 0.71 us
  matrix products: 13.7 us -> 0 us
  local copies, waits for them, and re-layouts: 5.12 us -> 16.1 us
  other arithmetic: 2.98 us -> 0 us
    all_gather x3 -> x0, blocking collectives: 94.3 us -> none  [the longest x1 32.2 us: body(): lax.all_gather(query_new.astype(jnp.bfloat16), 'fs', axis=0, tiled=True)]
    pallas_call x0 -> x1, Pallas kernels: none -> 62 us  [body(): pl.pallas_call(functools.partial(kernel, n, tp, chunks), out_shape=(sds((...]
    reduce_scatter x1 -> x0, waiting for transfers between devices: 60.7 us -> none  [body(): lax.psum_scatter((token_sum(upper_part, both_cotangents) + token_sum(lowe...]
    all_gather x1 -> x0, waiting for transfers between devices: 43.6 us -> none  [body(): factor_whole = lax.all_gather(row_factor, 'fs', axis=0, tiled=True)]
    psum x1 -> x0, blocking collectives: 40.3 us -> none  [body(): lax.psum((jnp.sum(query_dir * query_dir), jnp.sum(latent_dir * latent_dir...]
    dot_general x4 -> x0, matrix products: 13.7 us -> none  [the longest x1 9.51 us: body(): jnp.dot(normed_input, factor_whole, preferred_element_type=jnp.float32)]
    pallas_call x0 -> x3, local copies, waits for them, and re-layouts: none -> 5.75 us  [body(): pl.pallas_call(functools.partial(kernel, n, tp, chunks), out_shape=(sds((...]
    unnamed x30 -> x23, local copies, waits for them, and re-layouts: 5.12 us -> 10.3 us
  transfers between devices with their start and end apart: 2 -> 0, of which waited for: 2 -> 0; matrix products, arithmetic and copies ran while one was open for 1% -> 0% of each run, Pallas kernels for 0% -> 0%
where the time goes in v1:
time: 79.8 us; the launch traced here: 78.8 us
  Pallas kernels  62 us (78%)
  local copies, waits for them, and re-layouts  16.1 us (20%)
    pallas_call x1, Pallas kernels, body(): pl.pallas_call(functools.partial(kernel, n, tp, chunks), out_shape=(sds((...  62 us
    unnamed x23, local copies, waits for them, and re-layouts  10.3 us
    pallas_call x3, local copies, waits for them, and re-layouts, body(): pl.pallas_call(functools.partial(kernel, n, tp, chunks), out_shape=(sds((...  5.75 us

profile of v1, /device:TPU:0, one launch (start us, length us, event | category | flops | bytes accessed | tf_op | source)
XLA Modules:
  0.0 78.8 jit_solution(14084159862249653684)
XLA Ops:
  0.6 1.8 %copy.21.wq_ref = f32[256,192]{1,0:T(8,128)} copy(f32[256,192]{0,1:T(8,128)} %param.14) | data formatting | bytes 393216 | tf_op args[4]
  2.4 4.0 %copy.20 = bf16[4608,192]{1,0:T(8,128)(2,1)} copy(bf16[4608,192]{0,1:T(8,128)(2,1)} %param.11) | data formatting | bytes 3538944 | tf_op args[1]
  6.4 62.0 %shard_map.177 = (f32[256,192]{1,0:T(8,128)}, f32[256,128]{1,0:T(8,128)}, f32[256,192]{1,0:T(8,128)}, f32[256,128]{1,0:T(8,128)}, bf16[2048,192]{1,0:T(8,128)(2,...) custom-call(bf16[9,512,2048]{2,1,0:T(8,128)(2,1)} %bitcast.4, ...), custom_call_target="tpu_custom_call" | custom-call | tf_op jit(solution)/shard_map/pallas_call | solution.py:275
  68.4 0.0 copy-start.2
  68.4 0.0 copy-start.1
  68.4 0.0 copy-start
  68.4 0.0 copy-start.4
  68.4 0.0 copy-start.6
  68.4 0.0 copy-start.3
  68.4 0.0 copy-start.5
  68.4 1.8 %copy.22 = f32[256,192]{0,1:T(8,128)} copy(f32[256,192]{1,0:T(8,128)} %get-tuple-element.10) | data formatting | bytes 393216 | tf_op jit(solution)/shard_map/pallas_call | solution.py:275
  70.3 1.7 %copy.23 = f32[256,192]{0,1:T(8,128)} copy(f32[256,192]{1,0:T(8,128)} %get-tuple-element.12) | data formatting | bytes 393216 | tf_op jit(solution)/shard_map/pallas_call | solution.py:275
  72.0 2.2 %copy.24 = bf16[2048,192]{0,1:T(8,128)(2,1)} copy(bf16[2048,192]{1,0:T(8,128)(2,1)} %get-tuple-element.14) | data formatting | bytes 1572864 | tf_op jit(solution)/shard_map/pallas_call | solution.py:275
  74.2 0.0 copy-done.2
  74.2 0.7 copy.32
  74.8 0.0 copy-done.1
  74.8 0.7 copy.33
  75.5 0.0 copy-done
  75.5 0.8 %copy.34 = bf16[2048,128]{1,0:T(8,128)(2,1)} copy(bf16[2048,128]{1,0:T(8,128)(2,1)S(1)} %copy-done) | data formatting | bytes 1048576
  76.3 0.0 copy-done.4
  76.3 0.6 copy.35
  76.9 0.0 copy-done.6
  76.9 0.6 copy.36
  77.5 0.0 copy-done.3
  77.5 0.6 copy.37
  78.1 0.0 copy-done.5
  78.1 0.6 copy.38
Async XLA Ops:
  68.4 5.8 %copy-start.2 = (f32[256,128]{1,0:T(8,128)S(1)}, f32[256,128]{1,0:T(8,128)}, u32[]{:S(2)}) copy-start(f32[256,128]{1,0:T(8,128)} %get-tuple-element.31) | copy-start | bytes 393220
  68.4 6.5 %copy-start.1 = (f32[256,128]{1,0:T(8,128)S(1)}, f32[256,128]{1,0:T(8,128)}, u32[]{:S(2)}) copy-start(f32[256,128]{1,0:T(8,128)} %get-tuple-element.33) | copy-start | bytes 393220
  68.4 7.1 %copy-start = (bf16[2048,128]{1,0:T(8,128)(2,1)S(1)}, bf16[2048,128]{1,0:T(8,128)(2,1)}, u32[]{:S(2)}) copy-start(bf16[2048,128]{1,0:T(8,128)(2,1)} %get-tuple-element.35) | copy-start | bytes 1572868
  68.4 7.9 %copy-start.4 = (f32[32,192]{1,0:T(8,128)S(1)}, f32[32,192]{1,0:T(8,128)}, u32[]{:S(2)}) copy-start(f32[32,192]{1,0:T(8,128)} %get-tuple-element.36) | copy-start | bytes 73732
  68.4 8.5 %copy-start.6 = (f32[32,128]{1,0:T(8,128)S(1)}, f32[32,128]{1,0:T(8,128)}, u32[]{:S(2)}) copy-start(f32[32,128]{1,0:T(8,128)} %get-tuple-element.37) | copy-start | bytes 49156
  68.4 9.1 %copy-start.3 = (f32[32,192]{1,0:T(8,128)S(1)}, f32[32,192]{1,0:T(8,128)}, u32[]{:S(2)}) copy-start(f32[32,192]{1,0:T(8,128)} %get-tuple-element.38) | copy-start | bytes 73732
  68.4 9.7 %copy-start.5 = (f32[32,128]{1,0:T(8,128)S(1)}, f32[32,128]{1,0:T(8,128)}, u32[]{:S(2)}) copy-start(f32[32,128]{1,0:T(8,128)} %get-tuple-element.39) | copy-start | bytes 49156

commit v2 on v1

v2 whole, which is shorter than its diff:
```python
import functools

import jax
import jax.numpy as jnp
from jax import lax
from jax.experimental import pallas as pl
from jax.experimental.pallas import tpu as pltpu
from jax.sharding import PartitionSpec as P

MESH = pl.DeviceIdType.MESH
F32 = jnp.float32
BF16 = jnp.bfloat16


def directions(total, qw, mq_ref, mk_ref, vq_ref, vk_ref):
    def update(part, first, second):
        first_new = 0.8 * first + 0.2 * part
        second_new = 0.9 * second + 0.1 * part * part
        return first_new, second_new, first_new / (jnp.sqrt(second_new) + 1e-08)

    return (
        update(total[:, :qw], mq_ref[...], vq_ref[...]),
        update(total[:, qw:], mk_ref[...], vk_ref[...]),
    )


def exchange(
    n,
    tp,
    chunks,
    x_hbm,
    cq_hbm,
    ck_hbm,
    p_hbm,
    wq_ref,
    wk_ref,
    mq_ref,
    mk_ref,
    vq_ref,
    vk_ref,
    pall,
    wqall,
    wkall,
    dall,
    sums,
    total_ref,
    xs,
    cqs,
    cks,
    acc,
    rs_mine,
    rs_send,
    rs_recv,
    x_sem,
    c_sem,
    p_local,
    p_send,
    p_recv,
    s_send,
    s_recv,
    w_send,
    w_recv,
    v_send,
    v_recv,
    rs_ssem,
    rs_rsem,
    d_send,
    d_recv,
    q_send,
    q_recv,
):
    f = lax.axis_index("fs")
    t = lax.axis_index("tp")
    depth = n // 2
    col, side = f // 2, f % 2
    half = t % 2
    sibling = t + 1 - 2 * half
    across = f + 1 - 2 * side
    me = f * tp + t
    qw = mq_ref.shape[1]
    rr = mq_ref.shape[0]
    rows = wk_ref.shape[0]
    chunk = xs.shape[1]

    barrier = pltpu.get_barrier_semaphore()
    for i in range(n):
        for j in range(tp):
            if i or j:
                pl.semaphore_signal(
                    barrier,
                    inc=1,
                    device_id=(lax.rem(f + i, n), lax.rem(t + j, tp)),
                    device_id_type=MESH,
                )

    p_copy = pltpu.make_async_copy(p_hbm, pall.at[f], p_local)
    p_copy.start()
    cq_copy = pltpu.make_async_copy(cq_hbm, cqs, c_sem.at[0])
    ck_copy = pltpu.make_async_copy(ck_hbm, cks, c_sem.at[1])
    cq_copy.start()
    ck_copy.start()

    def x_copy(i):
        return pltpu.make_async_copy(x_hbm.at[i], xs.at[i], x_sem.at[i])

    for i in range(chunks):
        x_copy(i).start()

    wqall[f] = wq_ref[...].astype(BF16)
    wkall[f] = wk_ref[...].astype(BF16)
    acc[...] = jnp.zeros_like(acc)

    def remote(src, dst, ssem, rsem, to):
        return pltpu.make_async_remote_copy(
            src_ref=src, dst_ref=dst, send_sem=ssem, recv_sem=rsem, device_id=to, device_id_type=MESH
        )

    def p_fs(block, slot, to):
        ref = pall.at[block, half]
        return remote(ref, ref, p_send.at[slot], p_recv.at[block], (to, t))

    def p_tp(block, slot):
        ref = pall.at[block, half]
        return remote(ref, ref, s_send.at[slot], s_recv.at[block], (f, sibling))

    def w_fs(block, slot, to):
        q, v = wqall.at[block], wkall.at[block]
        return (
            remote(q, q, w_send.at[slot], w_recv.at[block], (to, t)),
            remote(v, v, v_send.at[slot], v_recv.at[block], (to, t)),
        )

    def w_go(block, slot, to):
        for copy in w_fs(block, slot, to):
            go(copy)

    def w_wait(block):
        for copy in w_fs(block, 0, across):
            copy.wait_recv()

    def column(k):
        return lax.rem(col + k, depth) * 2 + side

    def other(k):
        return lax.rem(col + k, depth) * 2 + 1 - side

    sends = []

    def go(copy):
        copy.start()
        sends.append(copy)

    def multiply(i, carry):
        x_copy(i).wait()
        at = pl.ds(pl.multiple_of(i * chunk, chunk), chunk)
        left = jnp.concatenate([cqs[:, at], cks[i].T], axis=0)
        acc[...] += jnp.dot(left, xs[i], preferred_element_type=F32)
        return carry

    p_copy.wait()
    pl.semaphore_wait(barrier, n * tp - 1)
    for k in range(1, depth):
        go(p_fs(f, k - 1, column(k)))
    go(p_fs(f, depth - 1, across))
    w_go(f, 0, across)
    near = sorted({k for k in (1, depth - 1) if 0 < k < depth})
    far = [k for k in range(1, depth) if k not in near]
    for k in near:
        w_go(f, k, column(k))

    cq_copy.wait()
    ck_copy.wait()
    first = (2 * chunks) // 3
    lax.fori_loop(0, first, multiply, 0)
    slot = depth
    for k in range(depth - 1, 0, -1):
        block = column(k)
        p_fs(block, 0, across).wait_recv()
        go(p_fs(block, slot, across))
        slot += 1
        go(p_tp(block, k))
    lax.fori_loop(first, chunks, multiply, 0)
    for k in range(depth):
        block = other(k)
        p_fs(block, 0, across).wait_recv()
        go(p_tp(block, depth + k))
    for k in range(depth):
        if k > 0:
            remote(pall.at[column(k), 1 - half], pall.at[column(k), 1 - half], s_send.at[0], s_recv.at[column(k)], (f, sibling)).wait_recv()
        remote(pall.at[other(k), 1 - half], pall.at[other(k), 1 - half], s_send.at[0], s_recv.at[other(k)], (f, sibling)).wait_recv()

    whole_p = pall[...].reshape(n * rows, pall.shape[-1])
    projected = jnp.dot(acc[...].astype(BF16), whole_p, preferred_element_type=F32).T
    for k in range(n):
        piece = projected[k * rr : (k + 1) * rr]
        rs_mine[k] = piece
        rs_send[k] = piece.astype(BF16)
    for k in range(1, n):
        to = lax.rem(f + k, n)
        go(remote(rs_send.at[to], rs_recv.at[f], rs_ssem.at[k], rs_rsem.at[f], (to, t)))
    for k in far:
        w_go(f, k, column(k))
    for k in near:
        block = column(depth - k)
        w_wait(block)
        w_go(block, depth + k, across)
    total = rs_mine[f]
    for k in range(1, n):
        src = lax.rem(f + n - k, n)
        remote(rs_recv.at[src], rs_recv.at[src], rs_ssem.at[0], rs_rsem.at[src], (f, sibling)).wait_recv()
        total = total + rs_recv[src].astype(F32)

    total_ref[...] = total
    (_, _, dir_q), (_, _, dir_k) = directions(total, qw, mq_ref, mk_ref, vq_ref, vk_ref)
    dall[f] = jnp.concatenate([dir_q, dir_k], axis=1).astype(BF16)
    lane = lax.broadcasted_iota(jnp.int32, (1, 128), 1)
    sums[me] = jnp.where(lane < 64, jnp.sum(dir_q * dir_q), jnp.sum(dir_k * dir_k))
    for k in range(1, n):
        to = lax.rem(f + k, n)
        go(remote(dall.at[f], dall.at[f], d_send.at[k], d_recv.at[f], (to, t)))
    for i in range(n):
        for j in range(tp):
            if i or j:
                to = (lax.rem(f + i, n), lax.rem(t + j, tp))
                go(remote(sums.at[me], sums.at[me], q_send.at[i * tp + j], q_recv.at[me], to))

    for k in far:
        block = column(depth - k)
        w_wait(block)
        w_go(block, depth + k, across)
    for k in range(1, n):
        src = lax.rem(f + n - k, n)
        remote(dall.at[src], dall.at[src], d_send.at[0], d_recv.at[src], (f, sibling)).wait_recv()
    for i in range(n):
        for j in range(tp):
            if i or j:
                src = lax.rem(f + i, n) * tp + lax.rem(t + j, tp)
                remote(sums.at[src], sums.at[src], q_send.at[0], q_recv.at[src], (f, sibling)).wait_recv()
    for k in range(depth):
        w_wait(other(k))
    for copy in sends:
        copy.wait_send()


def finish(
    n,
    tp,
    pall,
    wqall,
    wkall,
    dall,
    sums,
    total_ref,
    wq_ref,
    wk_ref,
    mq_ref,
    mk_ref,
    vq_ref,
    vk_ref,
    qnew_ref,
    knew_ref,
    qstep_ref,
    kstep_ref,
    qcopy_ref,
    kcopy_ref,
    qfirst_ref,
    kfirst_ref,
    qsecond_ref,
    ksecond_ref,
):
    f = lax.axis_index("fs")
    rr, qw = mq_ref.shape
    kw = mk_ref.shape[1]
    rows = wk_ref.shape[0]
    query, latent = directions(total_ref[...], qw, mq_ref, mk_ref, vq_ref, vk_ref)
    qfirst_ref[...], qsecond_ref[...] = query[:2]
    kfirst_ref[...], ksecond_ref[...] = latent[:2]
    row = jnp.sum(sums[...], axis=0)
    q_count = jnp.float32(n * rr * qw * tp)
    k_count = jnp.float32(n * rr * kw * tp)
    q_scale = 0.5 * jnp.sqrt(q_count) / jnp.sqrt(row[:, 0:1] + 1e-06)
    k_scale = 0.5 * jnp.sqrt(k_count) / jnp.sqrt(row[:, 64:65] + 1e-06)
    dirs = jnp.concatenate([dall[k].astype(F32) for k in range(n)], axis=0)
    left = dirs[:, :qw].T.astype(BF16)
    right = dirs[:, qw:].astype(BF16)

    def steps(factor):
        step_q = lax.dot_general(left, factor, (((1,), (1,)), ((), ())), preferred_element_type=F32)
        return step_q * q_scale, jnp.dot(factor, right, preferred_element_type=F32) * k_scale

    def block(i):
        return pall[i].reshape(rows, pall.shape[-1])

    step_q, step_k = steps(block(f))
    qstep_ref[...] = step_q
    kstep_ref[...] = step_k
    qnew_ref[...] = wq_ref[...] - step_q
    knew_ref[...] = wk_ref[...] - step_k
    for i in range(n):
        step_q, step_k = steps(block(i))
        at = slice(i * rows, (i + 1) * rows)
        qcopy_ref[:, at] = (wqall[i].astype(F32) - step_q).astype(BF16)
        kcopy_ref[at, :] = (wkall[i].astype(F32) - step_k).astype(BF16)


def solution(mesh):
    n, tp = mesh.shape["fs"], mesh.shape["tp"]

    def body(x, cq, ck, factor, wq, wk, mq, mk, vq, vk):
        tokens, width = x.shape
        rows, rank = factor.shape
        qw, kw = wq.shape[1], wk.shape[1]
        lat = qw + kw
        rr = mq.shape[0]
        chunk = 512
        while tokens % chunk:
            chunk //= 2
        chunks = tokens // chunk
        vmem = pl.BlockSpec(memory_space=pltpu.VMEM)
        anys = pl.BlockSpec(memory_space=pl.ANY)
        dma = pltpu.SemaphoreType.DMA
        sds = jax.ShapeDtypeStruct
        small = (wq.T, wk, mq, mk, vq, vk)
        params = pltpu.CompilerParams
        arrays = pl.pallas_call(
            functools.partial(exchange, n, tp, chunks),
            out_shape=(
                sds((n, 2, rows // 2, rank), BF16),
                sds((n, qw, rows), BF16),
                sds((n, rows, kw), BF16),
                sds((n, rr, lat), BF16),
                sds((n * tp, 1, 128), F32),
                sds((rr, lat), F32),
            ),
            in_specs=[anys] * 4 + [vmem] * 6,
            out_specs=(vmem,) * 6,
            scratch_shapes=[
                pltpu.VMEM((chunks, chunk, width), BF16),
                pltpu.VMEM((qw, tokens), BF16),
                pltpu.VMEM((chunks, chunk, kw), BF16),
                pltpu.VMEM((lat, width), F32),
                pltpu.VMEM((n, rr, lat), F32),
                pltpu.VMEM((n, rr, lat), BF16),
                pltpu.VMEM((n, rr, lat), BF16),
                dma((chunks,)),
                dma((2,)),
                dma(()),
            ]
            + [dma((n,))] * 12
            + [dma((n * tp,))] * 2,
            compiler_params=params(
                collective_id=0, has_side_effects=True, vmem_limit_bytes=50 * 1024 * 1024
            ),
        )(
            x.reshape(chunks, chunk, width),
            cq.T,
            ck.reshape(chunks, chunk, kw),
            factor.reshape(2, rows // 2, rank),
            *small,
        )
        out = pl.pallas_call(
            functools.partial(finish, n, tp),
            out_shape=(
                sds((qw, rows), F32),
                sds((rows, kw), F32),
                sds((qw, rows), F32),
                sds((rows, kw), F32),
                sds((qw, n * rows), BF16),
                sds((n * rows, kw), BF16),
                sds((rr, qw), F32),
                sds((rr, kw), F32),
                sds((rr, qw), F32),
                sds((rr, kw), F32),
            ),
            in_specs=[vmem] * 12,
            out_specs=(vmem,) * 10,
            compiler_params=params(vmem_limit_bytes=40 * 1024 * 1024),
        )(*arrays, *small)
        return (out[0].T, out[1], out[2].T, out[3], out[4].T) + tuple(out[5:])

    return jax.shard_map(
        body,
        mesh=mesh,
        in_specs=(P("fs", None), P("fs", "tp"), P("fs", "tp"), P("fs", None)) + (P("fs", "tp"),) * 6,
        out_specs=(P("fs", "tp"),) * 4 + (P(None, "tp"),) * 2 + (P("fs", "tp"),) * 4,
        check_vma=False,
    )
```

time: 79.8 us -> 52.5 us (0.66)
  Pallas kernels: 62 us -> 45.8 us
  local copies, waits for them, and re-layouts: 16.1 us -> 5.68 us
    pallas_call x1 -> x2, Pallas kernels: 62 us -> 45.8 us  [the longest x1 43.7 us: body(): pl.pallas_call(functools.partial(exchange, n, tp, chunks), out_shape=(sds...]
    pallas_call x3 -> x0, local copies, waits for them, and re-layouts: 5.75 us -> none  [body(): pl.pallas_call(functools.partial(kernel, n, tp, chunks), out_shape=(sds((...]
    unnamed x23 -> x14, local copies, waits for them, and re-layouts: 10.3 us -> 5.68 us
where the time goes in v2:
time: 52.5 us; the launch traced here: 52.1 us
  Pallas kernels  45.8 us (87%)
  local copies, waits for them, and re-layouts  5.68 us (11%)
  between operations  0.67 us (1%)
    pallas_call x1, Pallas kernels, body(): pl.pallas_call(functools.partial(exchange, n, tp, chunks), out_shape=(sds...  43.7 us
    unnamed x14, local copies, waits for them, and re-layouts  5.68 us
    pallas_call x1, Pallas kernels, body(): pl.pallas_call(functools.partial(finish, n, tp), out_shape=(sds((qw, rows...  2.12 us

profile of v2, /device:TPU:0, one launch (start us, length us, event | category | flops | bytes accessed | tf_op | source)
XLA Modules:
  0.0 52.1 jit_solution(6476938767686682783)
XLA Ops:
  0.6 0.0 copy-start
  0.7 0.9 %copy-done = f32[256,192]{0,1:T(8,128)S(1)} copy-done((f32[256,192]{0,1:T(8,128)S(1)}, f32[256,192]{0,1:T(8,128)}, u32[]{:S(2)}) %copy-start) | copy-done | bytes 196632
  1.6 0.0 copy-start.1
  1.6 0.9 %copy-done.1 = f32[256,128]{1,0:T(8,128)S(1)} copy-done((f32[256,128]{1,0:T(8,128)S(1)}, f32[256,128]{1,0:T(8,128)}, u32[]{:S(2)}) %copy-start.1) | copy-done | bytes 131096
  2.5 0.0 copy-start.2
  2.5 0.9 %copy-done.2 = bf16[256,256]{1,0:T(8,128)(2,1)S(1)} copy-done((bf16[256,256]{1,0:T(8,128)(2,1)S(1)}, bf16[256,256]{1,0:T(8,128)(2,1)}, u32[]{:S(2)}) %copy-start.2) | copy-done | bytes 131096
  3.4 0.0 copy-start.3
  3.4 0.8 %copy-done.3 = f32[32,192]{1,0:T(8,128)S(1)} copy-done((f32[32,192]{1,0:T(8,128)S(1)}, f32[32,192]{1,0:T(8,128)}, u32[]{:S(2)}) %copy-start.3) | copy-done | bytes 24600
  4.1 0.0 copy-start.4
  4.1 0.8 %copy-done.4 = f32[32,192]{1,0:T(8,128)S(1)} copy-done((f32[32,192]{1,0:T(8,128)S(1)}, f32[32,192]{1,0:T(8,128)}, u32[]{:S(2)}) %copy-start.4) | copy-done | bytes 24600
  4.9 0.0 copy-start.5
  4.9 0.7 %copy-done.5 = f32[32,128]{1,0:T(8,128)S(1)} copy-done((f32[32,128]{1,0:T(8,128)S(1)}, f32[32,128]{1,0:T(8,128)}, u32[]{:S(2)}) %copy-start.5) | copy-done | bytes 16408
  5.6 0.0 copy-start.6
  5.6 0.7 %copy-done.6 = f32[32,128]{1,0:T(8,128)S(1)} copy-done((f32[32,128]{1,0:T(8,128)S(1)}, f32[32,128]{1,0:T(8,128)}, u32[]{:S(2)}) %copy-start.6) | copy-done | bytes 16408
  6.3 43.7 %shard_map.177 = (bf16[8,2,128,256]{3,2,1,0:T(8,128)(2,1)S(1)}, bf16[8,192,256]{2,1,0:T(8,128)(2,1)S(1)}, bf16[8,256,128]{2,1,0:T(8,128)(2,1)S(1)}, bf16[8,32,32...) custom-call(bf16[9,512,2048]{2,1,0:T(8,128)(2,1)} %bitcast.11, bf16[192,4608]{1,0:T(8,128)(2,1)} %bitcast.12, ...), custom_call_target="tpu_custom_call" | custom-call | tf_op jit(solution)/shard_map/pallas_call | solution.py:325
  50.0 2.1 %shard_map.178 = (f32[192,256]{1,0:T(8,128)}, f32[256,128]{1,0:T(8,128)}, f32[192,256]{1,0:T(8,128)}, f32[256,128]{1,0:T(8,128)}, bf16[192,2048]{1,0:T(8,128)(2,...) custom-call(bf16[8,2,128,256]{3,2,1,0:T(8,128)(2,1)S(1)} %get-tuple-, ...), custom_call_target="tpu_custom_call" | custom-call | tf_op jit(solution)/shard_map/pallas_call | solution.py:361
Async XLA Ops:
  0.6 0.9 %copy-start = (f32[256,192]{0,1:T(8,128)S(1)}, f32[256,192]{0,1:T(8,128)}, u32[]{:S(2)}) copy-start(f32[256,192]{0,1:T(8,128)} %param.14) | copy-start | bytes 589828
  1.6 0.9 %copy-start.1 = (f32[256,128]{1,0:T(8,128)S(1)}, f32[256,128]{1,0:T(8,128)}, u32[]{:S(2)}) copy-start(f32[256,128]{1,0:T(8,128)} %wk_ref.3) | copy-start | bytes 393220
  2.5 0.9 %copy-start.2 = (bf16[256,256]{1,0:T(8,128)(2,1)S(1)}, bf16[256,256]{1,0:T(8,128)(2,1)}, u32[]{:S(2)}) copy-start(bf16[256,256]{1,0:T(8,128)(2,1)} %param.13) | copy-start | bytes 393220
  3.4 0.8 %copy-start.3 = (f32[32,192]{1,0:T(8,128)S(1)}, f32[32,192]{1,0:T(8,128)}, u32[]{:S(2)}) copy-start(f32[32,192]{1,0:T(8,128)} %mq_ref.3) | copy-start | bytes 73732
  4.1 0.8 %copy-start.4 = (f32[32,192]{1,0:T(8,128)S(1)}, f32[32,192]{1,0:T(8,128)}, u32[]{:S(2)}) copy-start(f32[32,192]{1,0:T(8,128)} %vq_ref.3) | copy-start | bytes 73732
  4.9 0.7 %copy-start.5 = (f32[32,128]{1,0:T(8,128)S(1)}, f32[32,128]{1,0:T(8,128)}, u32[]{:S(2)}) copy-start(f32[32,128]{1,0:T(8,128)} %mk_ref.3) | copy-start | bytes 49156
  5.6 0.7 %copy-start.6 = (f32[32,128]{1,0:T(8,128)S(1)}, f32[32,128]{1,0:T(8,128)}, u32[]{:S(2)}) copy-start(f32[32,128]{1,0:T(8,128)} %vk_ref.3) | copy-start | bytes 49156
